TPU v7x, 32 devices: a whole 2x2x4 slice. The times are simulated.
32 devices in a mesh: kv: 8 (over z, x), tp: 4 (over y, core).
Axes of the slice: x: 2, y: 2, z: 4, core: 2. Of those that a mesh axis runs over, the one named last changes fastest.
Arguments:
- activations: bfloat16 [384, 2048], P(None, ('kv', 'tp')), may hold values from -6 to 6
- latent_cache: bfloat16 [24, 16384, 288], P(None, 'kv'), may hold values from -6 to 6
- lengths: int32 [24], replicated, may hold values from 4096 to 16352, as said below
- accepted: int32 [24], replicated, may hold values from 0 to 16
- parents: int32 [24, 16], replicated, may hold values from -1 to 14, as said below
- w_query_down: bfloat16 [2048, 512], P(('kv', 'tp')), may hold values from -0.125 to 0.125
- w_key_down: bfloat16 [2048, 288], P(('kv', 'tp')), may hold values from -0.125 to 0.125
- gain_input: bfloat16 [2048], P(('kv', 'tp')), may hold values from 0.099609375 to 1.8984375
- gain_query: bfloat16 [512], replicated, may hold values from 0.099609375 to 1.8984375
- gain_key: bfloat16 [256], replicated, may hold values from 0.099609375 to 1.8984375
- w_query: bfloat16 [512, 16, 288], P(None, 'tp'), as said below
- w_value: bfloat16 [16, 256, 64], replicated, may hold values from -0.375 to 0.375
- w_out: bfloat16 [1024, 2048], P('tp', 'kv'), may hold values from -1 to 1, as said below
- gain_output: bfloat16 [2048], P('kv'), may hold values from 0.099609375 to 1.8984375
Outputs:
- mixed: bfloat16 [384, 2048], P(None, 'kv')
- new_cache: bfloat16 [24, 16384, 288], P(None, 'kv')
Inputs may be any that keep to these rules, and one draw needn't show every extreme that they name: One sequence has lengths exactly 16352 and another exactly 4096; which ones varies. accepted is between 0 and 16, so the proposals' positions lie below 16384. `parents`: the parent of proposal i is -1 or a proposal with a smaller index; proposal 0 has parent -1; the proposals of exactly one sequence (which one varies) form a single chain; the other sequences' proposals form general trees. `w_query`: entries are normal with standard deviation (1536)^(-1/2) cut at six standard deviations; in the hidden draw the heads whose index is a multiple of 4 are 48 times larger. `w_out`: entries of order (1024)^(-1/2).
All inputs are finite; a program needn't handle non-finite values.
Results may differ from a plain program's by a relative error of at most 0.0096.
The roundings to bfloat16 on the way count: a program that leaves them out, or rounds other values in their place, can miss the bound.
Values may be sent and summed in bfloat16 or wider, within the bound.
A program may use at most 192 MiB of HBM per device.

v0:
```python
import jax
import jax.numpy as jnp
from jax import lax
from jax.sharding import PartitionSpec as P

D = 2048
ROPE_DIM = 32
NOPE_DIM = 64


epsilon = 1e-06
rope_base = 10000.0
score_after_mask = -1e30


def rotate(component, places):
    half_width = component.shape[-1] // 2
    frequency = rope_base ** (-jnp.arange(half_width, dtype=jnp.float32) / half_width)
    angles = places.astype(jnp.float32)[:, None] * frequency[None, :]
    target_shape = (places.shape[0],) + (1,) * (component.ndim - 2) + (half_width,)
    cosine = jnp.cos(angles).reshape(target_shape)
    sine_part = jnp.sin(angles).reshape(target_shape)
    front_half = component[..., :half_width]
    back_half = component[..., half_width:]
    return jnp.concatenate(
        [front_half * cosine - back_half * sine_part, back_half * cosine + front_half * sine_part],
        axis=-1,
    )


def normalize(values, scales):
    return (
        values
        * lax.rsqrt(jnp.mean(values * values, axis=-1, keepdims=True) + epsilon)
        * scales.astype(jnp.float32)
    )


def ancestry(parents):
    seq_count, prop_count = parents.shape
    slot_ids = jnp.arange(prop_count, dtype=jnp.int32)
    parent_links = (parents[:, :, None] == slot_ids[None, None, :]).astype(jnp.float32)
    identity = jnp.broadcast_to(jnp.eye(prop_count, dtype=jnp.float32), parent_links.shape)
    reached = jnp.minimum(identity + parent_links, 1.0)
    for repeat in range((prop_count - 1).bit_length()):
        reached = jnp.minimum(
            jnp.einsum("sij,sjk->sik", reached, reached, precision=lax.Precision.HIGHEST), 1.0
        )
    depths = (jnp.sum(reached, axis=-1) - 1.0).astype(jnp.int32)
    return (reached, depths)


def down_terms(features, gain_rows, query_down, key_down):
    as_float = features.astype(jnp.float32)
    scaled = (as_float * gain_rows.astype(jnp.float32)).astype(jnp.bfloat16)
    squares = jnp.sum(as_float * as_float, axis=-1)
    query_segment = jnp.dot(scaled, query_down, preferred_element_type=jnp.float32)
    key_segment = jnp.dot(scaled, key_down, preferred_element_type=jnp.float32)
    return (squares, query_segment, key_segment)


def partial_attend(queries, key_rows, slot_index, onehot, reached, kv_rank, value_locally):
    score_scale = (NOPE_DIM + ROPE_DIM) ** (-0.5)
    ancestors = jnp.einsum("sij,snj->sin", reached, onehot, precision=lax.Precision.HIGHEST)
    visible = ((slot_index < 0)[:, None, :] | (ancestors > 0.5))[:, :, None, :]
    scores = (
        jnp.einsum("siha,sna->sihn", queries, key_rows, preferred_element_type=jnp.float32)
        * score_scale
    )
    masked = jnp.where(visible, scores, score_after_mask)
    maxima = jnp.max(masked, axis=-1)
    weights = jnp.where(visible, jnp.exp(masked - maxima[..., None]), 0.0)
    totals = jnp.sum(weights, axis=-1)
    weighted = jnp.einsum(
        "sihn,snk->sihk",
        weights.astype(jnp.bfloat16),
        key_rows[:, :, :kv_rank],
        preferred_element_type=jnp.float32,
    )
    value_fraction = (weighted / jnp.maximum(totals, 1.0)[..., None]).astype(jnp.bfloat16)
    values = jnp.einsum(
        "pwmb,mbe->pwme", value_fraction, value_locally, preferred_element_type=jnp.float32
    )
    return (maxima, totals, values.astype(jnp.bfloat16))


def combine_parts(maxima, totals, values):
    largest = jnp.max(maxima, axis=0)
    shares = totals * jnp.exp(maxima - largest[None])
    summed = jnp.sum(shares[..., None] * values.astype(jnp.float32), axis=0)
    return (summed / jnp.sum(shares, axis=0)[..., None]).astype(jnp.bfloat16)


def local(
    activations,
    latent_cache,
    lengths,
    accepted,
    parents,
    w_query_down,
    w_key_down,
    gain_input,
    gain_query,
    gain_key,
    w_query,
    w_value,
    w_out,
    gain_output,
):
    seq_count, prop_count = parents.shape
    row_count = activations.shape[0]
    heads_here = w_query.shape[1]
    kv_rank = gain_key.shape[0]
    span_len = latent_cache.shape[1]
    reached, depths = ancestry(parents)
    filled = lengths + accepted
    places = (filled[:, None] + depths).reshape(-1)
    features, gain_rows, query_down, key_down = (
        lax.all_gather(activations, "tp", axis=1, tiled=True),
        lax.all_gather(gain_input, "tp", axis=0, tiled=True),
        lax.all_gather(w_query_down, "tp", axis=0, tiled=True),
        lax.all_gather(w_key_down, "tp", axis=0, tiled=True),
    )
    squares, query_segment, key_segment = down_terms(features, gain_rows, query_down, key_down)
    squares, query_raw, key_raw = lax.psum((squares, query_segment, key_segment), "kv")
    inverse = lax.rsqrt(squares / D + epsilon)[:, None]
    query_low = normalize(query_raw * inverse, gain_query).astype(jnp.bfloat16)
    key_full = key_raw * inverse
    mapped_output = jnp.dot(
        query_low, w_query.reshape(w_query.shape[0], -1), preferred_element_type=jnp.float32
    )
    mapped_output = mapped_output.reshape(row_count, heads_here, -1)
    queries = jnp.concatenate(
        [mapped_output[..., :kv_rank], rotate(mapped_output[..., kv_rank:], places)], axis=-1
    ).astype(jnp.bfloat16)
    fresh_rows = jnp.concatenate(
        [normalize(key_full[:, :kv_rank], gain_key), rotate(key_full[:, kv_rank:], places)], axis=-1
    ).astype(jnp.bfloat16)
    locations_held = lax.axis_index("kv") * span_len + jnp.arange(span_len, dtype=jnp.int32)
    slot_index = locations_held[None, :] - filled[:, None]
    onehot = slot_index[:, :, None] == jnp.arange(prop_count, dtype=jnp.int32)[None, None, :]
    fresh_block = fresh_rows.reshape(seq_count, prop_count, -1)
    placed = jnp.einsum(
        "snj,sja->sna", onehot.astype(jnp.bfloat16), fresh_block, preferred_element_type=jnp.float32
    ).astype(jnp.bfloat16)
    updated = jnp.where(jnp.any(onehot, axis=-1)[:, :, None], placed, latent_cache)
    head_start = lax.axis_index("tp") * heads_here
    value_locally = lax.dynamic_slice_in_dim(w_value, head_start, heads_here, 0)
    maxima, totals, values = partial_attend(
        queries.reshape(seq_count, prop_count, heads_here, -1),
        updated,
        slot_index,
        onehot.astype(jnp.float32),
        reached,
        kv_rank,
        value_locally,
    )
    maxima = maxima.reshape(1, row_count, heads_here)
    totals = totals.reshape(1, row_count, heads_here)
    values = values.reshape(1, row_count, heads_here, -1)
    maxima, totals = (
        lax.all_gather(maxima, "kv", axis=0, tiled=True),
        lax.all_gather(totals, "kv", axis=0, tiled=True),
    )
    values = lax.all_gather(values, "kv", axis=0, tiled=True)
    attended = combine_parts(maxima, totals, values).reshape(row_count, -1)
    head_terms = jnp.dot(attended, w_out, preferred_element_type=jnp.float32)
    mixed_raw = lax.psum(head_terms, "tp")
    total_sq = lax.psum(jnp.sum(mixed_raw * mixed_raw, axis=-1), "kv")
    result = (
        mixed_raw * lax.rsqrt(total_sq / D + epsilon)[:, None] * gain_output.astype(jnp.float32)
    ).astype(jnp.bfloat16)
    return (result, updated)


def solution(mesh):
    in_specs = (
        P(None, ("kv", "tp")),
        P(None, "kv", None),
        P(),
        P(),
        P(),
        P(("kv", "tp"), None),
        P(("kv", "tp"), None),
        P(("kv", "tp")),
        P(),
        P(),
        P(None, "tp", None),
        P(),
        P("tp", "kv"),
        P("kv"),
    )
    out_specs = (P(None, "kv"), P(None, "kv", None))
    return jax.shard_map(local, mesh=mesh, in_specs=in_specs, out_specs=out_specs, check_vma=False)
```

profile of v0, /device:TPU:0, one launch (start us, length us, event | category | flops | bytes accessed | tf_op | source)
XLA Modules:
  0.0 322.6 jit_solution(7853236697493390630)
XLA Ops:
  7.2 1.3 dynamic-slice
  9.2 0.9 dynamic-update-slice
  10.1 8.4 %all-reduce = bf16[256]{0:T(256)(128)(2,1)S(1)} all-reduce(bf16[256]{0:T(256)(128)(2,1)S(1)} %dynamic-update-slice), channel_id=1, replica_groups=mesh['kv'=8,'tp'=4] {'tp'}, use_global_device_ids=true, to_apply=%add | all-reduce | flops 256 | bytes 1024
  18.5 5.8 %all_gather.21 = bf16[384,256]{0,1:T(8,128)(2,1)S(1)} all-gather(bf16[384,64]{0,1:T(8,128)(2,1)} %param.14), channel_id=1, replica_groups=mesh['kv'=8,'tp'=4] {'tp'}, dimensions={1}, use_global_device_ids=true | all-gather | bytes 245760 | tf_op jit(solution)/shard_map/all_gather | solution.py:119
  24.3 6.0 %all_gather.23 = bf16[256,512]{1,0:T(8,128)(2,1)S(1)} all-gather(bf16[64,512]{1,0:T(8,128)(2,1)} %param.19), channel_id=1, replica_groups=mesh['kv'=8,'tp'=4] {'tp'}, dimensions={0}, use_global_device_ids=true | all-gather | bytes 327680 | tf_op jit(solution)/shard_map/all_gather | solution.py:121
  30.3 5.8 %all_gather.24 = bf16[256,288]{1,0:T(8,128)(2,1)S(1)} all-gather(bf16[64,288]{1,0:T(8,128)(2,1)} %param.20), channel_id=1, replica_groups=mesh['kv'=8,'tp'=4] {'tp'}, dimensions={0}, use_global_device_ids=true | all-gather | bytes 184320 | tf_op jit(solution)/shard_map/all_gather | solution.py:122
  36.1 1.3 fusion.49
  37.4 1.1 fusion.47
  38.6 22.2 %psum.36 = f32[384]{0:T(512)S(1)} all-reduce(f32[384]{0:T(512)S(1)} %fusion.28), channel_id=1, replica_groups=mesh['kv'=8,'tp'=4] {'kv'}, use_global_device_ids=true, to_apply=%region_2.0 | all-reduce | flops 384 | bytes 3072 | tf_op jit(solution)/shard_map/psum | solution.py:125
  60.8 0.7 convert_element_type.91
  61.5 0.8 copy.38
  62.3 0.4 convolution_minimum_fusion.3
  62.7 0.3 convolution_minimum_fusion.2
  63.0 0.3 convolution_minimum_fusion.1
  63.3 0.4 fusion.60
  63.8 0.7 add.80
  64.7 0.7 convert_element_type.86
  65.4 1.5 fusion.12
  67.0 2.0 compare_or_fusion
  69.1 51.6 %all-reduce.7.cloned.1.call-done = (f32[384,288]{0,1:T(8,128)}, f32[384,512]{1,0:T(8,128)}) async-done(((f32[384,288]{0,1:T(8,128)}, f32[384,512]{1,0:T(8,128)}), (f32[384,288]{0,1:T(8,128)}, f32[384,512]{1,0:T(8,128)})) %all-reduce.7.cloned.1.call-update) | async-done | bytes 1228816 | tf_op jit(solution)/shard_map/psum | solution.py:125
  120.7 1.0 broadcast_multiply_fusion
  122.0 0.2 multiply_cosine_fusion
  122.2 0.7 copy.61
  123.0 0.7 copy.62
  123.7 1.4 multiply_reduce_fusion.1
  125.1 2.0 fusion.22
  127.3 0.3 concatenate.23
  127.6 0.3 copy.43
  127.9 0.3 concatenate.24
  128.3 0.3 copy.44
  128.6 0.3 copy.41
  128.9 25.2 %convert_select_fusion = bf16[24,2048,288]{1,2,0:T(8,128)(2,1)} fusion(bf16[24,2048,288]{1,2,0:T(8,128)(2,1)} %param.15, pred[24,2048]{1,0:T(8,128)(4,1)} %fusion.12, s32[24,2048]{1,0:T(8,128)S(1)} %broadcast_subtract_fusion, bf16[24,16,16]{2,1,0:T(8,128)(2,1)} %bitcast.62, bf16[24,16,16]{2,1,0:T(8,128)(2,1)} %bitcast.61, bf16[24,16,256]{2,1,0:T(8,128)(2,1)S(1)} %bitcast.60), kind=kOutput, calls=%fused_computation.2 | convolution fusion | flops 482746368 | bytes 57090048 | tf_op jit(solution)/shard_map/snj,sja->sna/dot_general | solution.py:143
  154.1 15.5 %fusion.3 = (f32[24,16,4]{1,2,0:T(4,128)S(1)}, f32[24,16,4,2048]{3,1,2,0:T(8,128)}) fusion(pred[24,16,2048]{2,1,0:T(8,128)(4,1)S(1)} %compare_or_fusion, bf16[24,2048,288]{1,2,0:T(8,128)(2,1)} %convert_select_fusion, bf16[24,16,4,16]{3,1,2,0:T(8,128)(2,1)S(1)} %copy.44, bf16[24,16,4,16]{3,1,2,0:T(8,128)(2,1)S(1)} %copy.43, ...), kind=kOutput, calls=%fused_computation.7 | convolution fusion | flops 1824029184 | bytes 42571776 | tf_op jit(solution)/shard_map/siha,sna->sihn/dot_general | solution.py:67
  169.6 6.9 %fusion.5 = f32[24,16,4]{1,2,0:T(4,128)S(1)} fusion(f32[24,16,4,2048]{3,1,2,0:T(8,128)} %get-tuple-element.17, f32[24,16,4]{1,2,0:T(4,128)S(1)} %get-tuple-element.16, pred[24,16,2048]{2,1,0:T(8,128)(4,1)S(1)} %compare_or_fusion), kind=kLoop, calls=%fused_computation.9 | loop fusion | flops 15727104 | bytes 13381632 | tf_op jit(solution)/shard_map/reduce_sum | solution.py:73
  176.5 15.1 %divide_convert_fusion = bf16[24,16,4,256]{3,1,2,0:T(8,128)(2,1)S(1)} fusion(bf16[24,2048,288]{1,2,0:T(8,128)(2,1)} %convert_select_fusion, f32[24,16,4,2048]{3,1,2,0:T(8,128)} %get-tuple-element.17, f32[24,16,4]{1,2,0:T(4,128)S(1)} %get-tuple-element.16, pred[24,16,2048]{2,1,0:T(8,128)(4,1)S(1)} %compare_or_fusion, f32[24,16,4]{1,2,0:T(4,128)S(1)} %broadcast_maximum_fusion), kind=kOutput, calls=%fused_computation.21 | convolution fusion | flops 1627127808 | bytes 39333888 | tf_op jit(solution)/shard_map/sihn,snk->sihk/dot_general | solution.py:74
  191.7 1.6 fusion.16
  193.4 0.8 copy.53
  194.5 30.7 %all_gather.26 = f32[8,384,4]{1,2,0:T(4,128)S(1)} all-gather(f32[1,384,4]{1,2,0:T(4,128)S(1)} %reshape.200), channel_id=1, replica_groups=mesh['kv'=8,'tp'=4] {'kv'}, dimensions={0}, use_global_device_ids=true | all-gather | bytes 55296 | tf_op jit(solution)/shard_map/all_gather | solution.py:162
  225.3 30.9 %all_gather.25 = f32[8,384,4]{1,2,0:T(4,128)S(1)} all-gather(f32[1,384,4]{1,2,0:T(4,128)S(1)} %reshape.199), channel_id=1, replica_groups=mesh['kv'=8,'tp'=4] {'kv'}, dimensions={0}, use_global_device_ids=true | all-gather | bytes 55296 | tf_op jit(solution)/shard_map/all_gather | solution.py:163
  256.2 1.8 multiply_reduce_fusion
  258.0 0.3 copy.65
  258.2 0.3 divide_convert_fusion.1
  258.5 0.2 copy.55
  258.7 1.0 fusion.61
  259.8 32.0 %all-reduce.5.cloned.1.call-done = f32[384,256]{1,0:T(8,128)} async-done(((f32[384,256]{1,0:T(8,128)}), f32[384,256]{1,0:T(8,128)}) %all-reduce.5.cloned.1.call-update) | async-done | bytes 393232 | tf_op jit(solution)/shard_map/psum | solution.py:168
  291.7 1.1 multiply_reduce_fusion.2
  292.9 21.4 %psum.39 = f32[384]{0:T(512)S(1)} all-reduce(f32[384]{0:T(512)S(1)} %multiply_reduce_fusion.2), channel_id=1, replica_groups=mesh['kv'=8,'tp'=4] {'kv'}, use_global_device_ids=true, to_apply=%region_15.16 | all-reduce | flops 384 | bytes 3072 | tf_op jit(solution)/shard_map/psum | solution.py:169
  314.2 1.8 multiply_convert_fusion.1
  (43 shorter events, 1.4 us)
Async XLA Ops:
  7.2 117.9 %copy-start = (bf16[512,4,288]{0,2,1:T(8,128)(2,1)S(1)}, bf16[512,4,288]{0,2,1:T(8,128)(2,1)}, u32[]{:S(2)}) copy-start(bf16[512,4,288]{0,2,1:T(8,128)(2,1)} %param.24) | copy-start | bytes 3538948
  7.2 113.5 %all-reduce.7.cloned.1.call-start = ((), (), s32[]{:S(2)}) async-start(), calls=%async_computation.2 | async-start | bytes 2457600 | tf_op jit(solution)/shard_map/psum | solution.py:125
  38.5 217.7 %all-gather.2.cloned.1.call-start = ((), (), s32[]{:S(2)}) async-start(), calls=%async_computation | async-start | bytes 1769472 | tf_op jit(solution)/shard_map/all_gather | solution.py:165
  176.5 82.2 %copy-start.2 = (bf16[256,256]{1,0:T(8,128)(2,1)S(1)}, bf16[256,256]{1,0:T(8,128)(2,1)}, u32[]{:S(2)}) copy-start(bf16[256,256]{1,0:T(8,128)(2,1)} %param.26) | copy-start | bytes 393220
  176.5 83.2 %copy-start.3 = (bf16[256]{0:T(256)(128)(2,1)S(1)}, bf16[256]{0:T(256)(128)(2,1)}, u32[]{:S(2)}) copy-start(bf16[256]{0:T(256)(128)(2,1)} %param.27) | copy-start | bytes 1540
  176.5 139.5 %copy-start.1 = (bf16[512,4,288]{0,2,1:T(8,128)(2,1)S(1)}, bf16[512,4,288]{0,2,1:T(8,128)(2,1)}, u32[]{:S(2)}) copy-start(bf16[512,4,288]{0,2,1:T(8,128)(2,1)} %param.24) | copy-start | bytes 3538948
  194.2 97.5 %all-reduce.5.cloned.1.call-start = ((), (), s32[]{:S(2)}) async-start(), calls=%async_computation.1 | async-start | bytes 786432 | tf_op jit(solution)/shard_map/psum | solution.py:168
Sparse Core Ops, SparseCore 0:
  38.6 81.9 all-reduce.6
  194.4 43.4 all-gather.1
  259.9 31.8 all-reduce.4
where the time goes:
time: 323 us
  blocking collectives  131 us (41%)
  waiting for transfers between devices  83.6 us (26%)
  matrix products  66.4 us (21%)
  other arithmetic  18.6 us (6%)
  between operations  14.7 us (5%)
  local copies, waits for them, and re-layouts  7.89 us (2%)
    psum x1, waiting for transfers between devices, local(): lax.psum((squares, query_segment, key_segment), 'kv')  51.6 us
    psum x1, waiting for transfers between devices, local(): mixed_raw = lax.psum(head_terms, 'tp')  32 us
    all_gather x1, blocking collectives, local(): lax.all_gather(totals, 'kv', axis=0, tiled=True)  30.9 us
    all_gather x1, blocking collectives, local(): lax.all_gather(maxima, 'kv', axis=0, tiled=True)  30.7 us
    dot_general x1, matrix products, local(): jnp.einsum('snj,sja->sna', onehot.astype(jnp.bfloat16), fresh_block, pref...  25.2 us
    psum x1, blocking collectives, local(): lax.psum((squares, query_segment, key_segment), 'kv')  22.2 us
    psum x1, blocking collectives, local(): total_sq = lax.psum(jnp.sum(mixed_raw * mixed_raw, axis=-1), 'kv')  21.4 us
    dot_general x1, matrix products, partial_attend(): jnp.einsum('siha,sna->sihn', queries, key_rows, preferred_element_type=jn...  15.5 us
  transfers between devices with their start and end apart: 3, of which 2 were waited for; matrix products, arithmetic and copies ran while one was open for 3% of the time, Pallas kernels for 0%

commit v1 on v0

v1 whole, which is shorter than its diff:
```python
import functools

import jax
import jax.numpy as jnp
from jax import lax
from jax.experimental import pallas as pl
from jax.experimental.pallas import tpu as pltpu
from jax.sharding import PartitionSpec as P

NOPE_DIM = 64
LANES = 128

epsilon = 1e-06
rope_base = 10000.0
score_after_mask = -1e30
MESH = pl.DeviceIdType.MESH
HIGHEST = lax.Precision.HIGHEST
VMEM = pl.BlockSpec(memory_space=pltpu.VMEM)


def ancestry(parents):
    seq_count, prop_count = parents.shape
    slot_ids = jnp.arange(prop_count, dtype=jnp.int32)
    parent_links = (parents[:, :, None] == slot_ids[None, None, :]).astype(jnp.bfloat16)
    identity = jnp.broadcast_to(jnp.eye(prop_count, dtype=jnp.bfloat16), parent_links.shape)
    reached = jnp.minimum(identity + parent_links, 1.0)
    for repeat in range((prop_count - 1).bit_length()):
        reached = jnp.minimum(
            jnp.einsum("sij,sjk->sik", reached, reached, preferred_element_type=jnp.float32), 1.0
        ).astype(jnp.bfloat16)
    depths = (jnp.sum(reached.astype(jnp.float32), axis=-1) - 1.0).astype(jnp.int32)
    return (reached, depths)


def dot(a, b, precision=None):
    return jnp.dot(a, b, preferred_element_type=jnp.float32, precision=precision)


def dot_nt(a, b, precision=None):
    return lax.dot_general(
        a, b, (((1,), (1,)), ((), ())), preferred_element_type=jnp.float32, precision=precision
    )


def remote(src, dst, send_sem, recv_sem, device_id):
    return pltpu.make_async_remote_copy(
        src_ref=src,
        dst_ref=dst,
        send_sem=send_sem,
        recv_sem=recv_sem,
        device_id=device_id,
        device_id_type=MESH,
    )


def root_mean(values, count):
    return lax.rsqrt(jnp.sum(values * values, axis=-1, keepdims=True) / count + epsilon)


def compress_kernel(
    n_kv, n_tp, width, q_rank, kv_rank, turn_dim,
    x_ref, w_ref, cos_ref, sin_ref, gain_q_ref, gain_k_ref, out_ref,
    got_x, got_w, part, got_part, all_rows,
    send_x, recv_x, send_w, recv_w, send_p, recv_p, send_a, send_b, recv_a,
):
    me_k, me_t = lax.axis_index("kv"), lax.axis_index("tp")
    barrier = pltpu.get_barrier_semaphore()
    for dk in range(n_kv):
        for dt in range(n_tp):
            if dk or dt:
                pl.semaphore_signal(
                    barrier,
                    inc=1,
                    device_id={"kv": lax.rem(me_k + dk, n_kv), "tp": lax.rem(me_t + dt, n_tp)},
                    device_id_type=MESH,
                )
    pl.semaphore_wait(barrier, n_kv * n_tp - 1)

    sends = []
    features = w_ref.shape[0]
    for d in range(1, n_tp):
        peer = lax.rem(me_t + d, n_tp)
        for src, dst, ss, rs in (
            (x_ref.at[peer], got_x.at[me_t], send_x.at[d], recv_x.at[me_t]),
            (w_ref, got_w.at[me_t], send_w.at[d], recv_w.at[me_t]),
        ):
            copy = remote(src, dst, ss, rs, {"tp": peer})
            copy.start()
            sends.append(copy)

    def term(x, w):
        raw = x[:, features:].astype(jnp.float32)
        return dot(x[:, :features], w), jnp.sum(raw * raw, axis=-1, keepdims=True)

    total, squares = term(x_ref[me_t], w_ref[...])
    for d in range(1, n_tp):
        peer = lax.rem(me_t + d, n_tp)
        remote(x_ref.at[peer], got_x.at[peer], send_x.at[d], recv_x.at[peer], {"tp": peer}).wait_recv()
        remote(w_ref, got_w.at[peer], send_w.at[d], recv_w.at[peer], {"tp": peer}).wait_recv()
        more, more_squares = term(got_x[peer], got_w[peer])
        total, squares = total + more, squares + more_squares
    lane = lax.broadcasted_iota(jnp.int32, total.shape, 1)
    total = jnp.where(lane == width - 1, squares, total)
    each = part.shape[1]
    for j in range(n_kv):
        part[j] = total[j * each : (j + 1) * each]

    for d in range(1, n_kv):
        peer = lax.rem(me_k + d, n_kv)
        copy = remote(part.at[peer], got_part.at[me_k], send_p.at[d], recv_p.at[me_k], {"kv": peer})
        copy.start()
        sends.append(copy)
    summed = part[me_k]
    for d in range(1, n_kv):
        peer = lax.rem(me_k + d, n_kv)
        remote(
            part.at[peer], got_part.at[peer], send_p.at[d], recv_p.at[peer], {"kv": peer}
        ).wait_recv()
        summed = summed + got_part[peer]
    model = n_kv * n_tp * features
    inverse = lax.rsqrt(summed[:, width - 1 : width] / model + epsilon)
    query = summed[:, :q_rank] * inverse
    query = query * root_mean(query, q_rank) * gain_q_ref[...]
    latent = summed[:, q_rank : q_rank + kv_rank] * inverse
    latent = latent * root_mean(latent, kv_rank) * gain_k_ref[...]
    turn = summed[:, q_rank + kv_rank :] * inverse
    tail = turn.shape[1]
    swapped = pltpu.roll(turn, tail - turn_dim, 1)
    turned = turn * cos_ref[...] + swapped * sin_ref[...]
    mine = me_t * n_kv + me_k
    all_rows[mine, :, :q_rank] = query.astype(jnp.bfloat16)
    all_rows[mine, :, q_rank : q_rank + kv_rank] = latent.astype(jnp.bfloat16)
    all_rows[mine, :, q_rank + kv_rank :] = turned.astype(jnp.bfloat16)

    sibling = me_t + 1 - 2 * lax.rem(me_t, 2)
    peers = []
    for dy in range(n_tp // 2):
        for dk in range(n_kv):
            if dy or dk:
                peers.append((lax.rem(me_k + dk, n_kv), lax.rem(me_t + 2 * dy, n_tp)))
    for index, (pk, pt) in enumerate(peers):
        copy = remote(
            all_rows.at[mine], all_rows.at[mine], send_a.at[index], recv_a.at[mine],
            {"kv": pk, "tp": pt},
        )
        copy.start()
        sends.append(copy)

    def pass_on(index, block):
        copy = remote(
            all_rows.at[block], all_rows.at[block], send_b.at[index], recv_a.at[block],
            {"tp": sibling},
        )
        copy.start()
        sends.append(copy)

    pass_on(len(peers), mine)
    for index, (pk, pt) in enumerate(peers):
        block = pt * n_kv + pk
        remote(
            all_rows.at[block], all_rows.at[block], send_a.at[index], recv_a.at[block],
            {"kv": pk, "tp": pt},
        ).wait_recv()
        pass_on(index, block)
    for dy in range(n_tp // 2):
        for dk in range(n_kv):
            block = lax.rem(sibling + 2 * dy, n_tp) * n_kv + lax.rem(me_k + dk, n_kv)
            remote(
                all_rows.at[block], all_rows.at[block], send_b.at[0], recv_a.at[block],
                {"tp": sibling},
            ).wait_recv()
    out_ref[...] = all_rows[...]
    for copy in sends:
        copy.wait_send()


def attend_kernel(
    group, rel_ref, low_ref, wq_ref, cos_ref, sin_ref, reached_ref, fresh_ref, cache_ref,
    out_ref, part_ref, stats_ref, q_main, q_turn,
):
    heads, whole, _ = wq_ref.shape
    turn_dim = q_turn.shape[-1]
    rank = whole - turn_dim
    half = turn_dim // 2
    props = reached_ref.shape[-1]
    seqs = q_main.shape[0]
    span = cache_ref.shape[-1]
    step = pl.program_id(0)
    scale = (NOPE_DIM + turn_dim) ** (-0.5)

    @pl.when(step == 0)
    def _():
        low = low_ref[...]
        for h in range(heads):
            main = dot_nt(low, wq_ref[h, :rank, :])
            front, back = wq_ref[h, rank : rank + half, :], wq_ref[h, rank + half :, :]
            turn = dot_nt(low, jnp.concatenate([front, back], axis=0))
            swapped = dot_nt(low, jnp.concatenate([back, front], axis=0))
            turned = turn * cos_ref[...] + swapped * sin_ref[...]
            rows = slice(h * props, (h + 1) * props)
            q_main[:, rows, :] = main.astype(jnp.bfloat16).reshape(seqs, props, rank)
            q_turn[:, rows, :] = turned.astype(jnp.bfloat16).reshape(seqs, props, turn_dim)

    for g in range(group):
        s = step * group + g
        rel = rel_ref[s]
        out_ref[g] = cache_ref[g]
        first = lax.shift_right_arithmetic(rel, 7)
        for more in range(2):
            chunk = first + more

            @pl.when((chunk >= 0) & (chunk < span // LANES))
            def _():
                start = pl.multiple_of(chunk * LANES, LANES)
                slot = start - rel + lax.broadcasted_iota(jnp.int32, (props, LANES), 1)
                onehot = slot == lax.broadcasted_iota(jnp.int32, (props, LANES), 0)
                placed = dot(fresh_ref[g], onehot.astype(jnp.float32).astype(jnp.bfloat16))
                slots = start - rel + lax.broadcasted_iota(jnp.int32, placed.shape, 1)
                old = out_ref[g, :, pl.ds(start, LANES)].astype(jnp.float32)
                new = jnp.where((slots >= 0) & (slots < props), placed, old)
                out_ref[g, :, pl.ds(start, LANES)] = new.astype(jnp.bfloat16)

        slot = lax.broadcasted_iota(jnp.int32, (props, span), 1) - rel
        onehot = slot == lax.broadcasted_iota(jnp.int32, (props, span), 0)
        ancestors = dot(reached_ref[g], onehot.astype(jnp.float32).astype(jnp.bfloat16))
        bias = jnp.where((slot < 0) | (ancestors > 0.5), 0.0, score_after_mask)
        scores = dot(q_main[s], out_ref[g, :rank, :]) + dot(q_turn[s], out_ref[g, rank:, :])
        masked = scores.reshape(heads, props, span) * scale + bias[None]
        top = jnp.max(masked, axis=-1, keepdims=True)
        weights = jnp.exp(masked - jnp.maximum(top, -1e29))
        totals = jnp.sum(weights, axis=-1, keepdims=True)
        prob = weights.astype(jnp.bfloat16).reshape(heads * props, span)
        weighted = dot_nt(prob, out_ref[g, :rank, :]).reshape(heads, props, rank)
        part = (weighted / jnp.maximum(totals, 1.0)).astype(jnp.bfloat16)
        lane = lax.broadcasted_iota(jnp.int32, (props, LANES), 1)
        stats = jnp.zeros((props, LANES), jnp.float32)
        rows = slice(g * props, (g + 1) * props)
        for h in range(heads):
            part_ref[h, rows, :] = part[h]
            stats = jnp.where(lane == h, top[h], stats)
            stats = jnp.where(lane == heads + h, totals[h], stats)
        stats_ref[rows, :] = stats


def project_kernel(
    n_kv, n_tp,
    part_ref, stats_ref, wv_ref, w_out_ref, gain_ref, out_ref,
    vals, stat, got_vals, got_stat, attended, raw, got_raw, sums, result,
    send_v, recv_v, send_s, recv_s, send_a, recv_a, send_r, recv_r, send_q, recv_q, send_o, recv_o,
):
    me_k, me_t = lax.axis_index("kv"), lax.axis_index("tp")
    heads, _, _ = part_ref.shape
    v_dim = wv_ref.shape[1]
    kv_peers = [lax.rem(me_k + d, n_kv) for d in range(n_kv)]
    tp_peers = [lax.rem(me_t + d, n_tp) for d in range(n_tp)]
    barrier = pltpu.get_barrier_semaphore()
    for peer in kv_peers[1:]:
        pl.semaphore_signal(barrier, inc=1, device_id={"kv": peer}, device_id_type=MESH)
    for peer in tp_peers[1:]:
        pl.semaphore_signal(barrier, inc=1, device_id={"tp": peer}, device_id_type=MESH)
    sends = []

    each = vals.shape[1]
    values = jnp.concatenate([dot_nt(part_ref[h], wv_ref[h]) for h in range(heads)], axis=1)
    for j in range(n_kv):
        vals[j] = values[j * each : (j + 1) * each].astype(jnp.bfloat16)
        stat[j] = stats_ref[j * each : (j + 1) * each, :]
    pl.semaphore_wait(barrier, n_kv + n_tp - 2)

    def exchange(axis, peers, src_of, dst, own, send_sem, recv_sem):
        for d in range(1, len(peers)):
            copy = remote(
                src_of(peers[d]), dst.at[own], send_sem.at[d], recv_sem.at[own], {axis: peers[d]}
            )
            copy.start()
            sends.append(copy)

    def arrived(axis, peers, d, src_of, dst, send_sem, recv_sem):
        remote(
            src_of(peers[d]), dst.at[peers[d]], send_sem.at[d], recv_sem.at[peers[d]],
            {axis: peers[d]},
        ).wait_recv()

    exchange("kv", kv_peers, lambda p: stat.at[p], got_stat, me_k, send_s, recv_s)
    exchange("kv", kv_peers, lambda p: vals.at[p], got_vals, me_k, send_v, recv_v)
    for d in range(1, n_kv):
        arrived("kv", kv_peers, d, lambda p: stat.at[p], got_stat, send_s, recv_s)
    all_stats = [stat[me_k]] + [got_stat[p] for p in kv_peers[1:]]
    largest = all_stats[0]
    for one in all_stats[1:]:
        largest = jnp.maximum(largest, one)
    wide = lax.broadcasted_iota(jnp.int32, (each, heads * v_dim), 1)

    def spread(share):
        out = share[:, 0:1]
        for h in range(1, heads):
            out = jnp.where(wide >= h * v_dim, share[:, h : h + 1], out)
        return jnp.broadcast_to(out, wide.shape)

    summed = None
    for d in range(n_kv):
        one = all_stats[d]
        share = pltpu.roll(one, LANES - heads, 1) * jnp.exp(
            jnp.minimum(one - largest, 0.0)
        )
        share = spread(share)
        if d:
            arrived("kv", kv_peers, d, lambda p: vals.at[p], got_vals, send_v, recv_v)
        block = got_vals[kv_peers[d]] if d else vals[me_k]
        term = share * block.astype(jnp.float32)
        summed = term if summed is None else summed + term
        weight = share if d == 0 else weight + share
    attended[me_k] = (summed / weight).astype(jnp.bfloat16)
    exchange("kv", kv_peers, lambda p: attended.at[me_k], attended, me_k, send_a, recv_a)
    for d in range(1, n_kv):
        arrived("kv", kv_peers, d, lambda p: attended.at[p], attended, send_a, recv_a)

    lines = jnp.concatenate([attended[j].astype(jnp.float32) for j in range(n_kv)], axis=0)
    lines = dot(lines.astype(jnp.bfloat16), w_out_ref[...])
    share_rows = raw.shape[1]
    for t in range(n_tp):
        raw[t] = lines[t * share_rows : (t + 1) * share_rows]
    exchange("tp", tp_peers, lambda p: raw.at[p], got_raw, me_t, send_r, recv_r)
    mixed = raw[me_t]
    for d in range(1, n_tp):
        arrived("tp", tp_peers, d, lambda p: raw.at[p], got_raw, send_r, recv_r)
        mixed = mixed + got_raw[tp_peers[d]]
    cols = mixed.shape[1]
    sums[me_k] = dot_nt(jnp.ones((8, cols), jnp.float32), mixed * mixed, HIGHEST)
    exchange("kv", kv_peers, lambda p: sums.at[me_k], sums, me_k, send_q, recv_q)
    for d in range(1, n_kv):
        arrived("kv", kv_peers, d, lambda p: sums.at[p], sums, send_q, recv_q)
    square = sums[0]
    for j in range(1, n_kv):
        square = square + sums[j]
    norm = lax.rsqrt(square / (cols * n_kv) + epsilon)
    eye = lax.broadcasted_iota(jnp.int32, (share_rows, share_rows), 0) == lax.broadcasted_iota(
        jnp.int32, (share_rows, share_rows), 1
    )
    column = dot_nt(eye.astype(jnp.float32), norm, HIGHEST)
    result[me_t] = (mixed * column[:, 0:1] * gain_ref[...]).astype(jnp.bfloat16)
    exchange("tp", tp_peers, lambda p: result.at[me_t], result, me_t, send_o, recv_o)
    for d in range(1, n_tp):
        arrived("tp", tp_peers, d, lambda p: result.at[p], result, send_o, recv_o)
    out_ref[...] = result[...]
    for copy in sends:
        copy.wait_send()


def up(value, to):
    return -(-value // to) * to


def local(
    n_kv,
    n_tp,
    activations,
    latent_cache,
    lengths,
    accepted,
    parents,
    w_query_down,
    w_key_down,
    gain_input,
    gain_query,
    gain_key,
    w_query,
    w_value,
    w_out,
    gain_output,
):
    bf16, f32 = jnp.bfloat16, jnp.float32
    seqs, props = parents.shape
    rows, features = activations.shape
    heads = w_query.shape[1]
    q_rank, kv_rank = gain_query.shape[0], gain_key.shape[0]
    whole = latent_cache.shape[-1]
    turn_dim = whole - kv_rank
    half = turn_dim // 2
    span = latent_cache.shape[1]
    v_dim = w_value.shape[-1]
    cols = w_out.shape[1]
    n_dev = n_kv * n_tp
    me_k, me_t = lax.axis_index("kv"), lax.axis_index("tp")

    reached, depths = ancestry(parents)
    filled = lengths + accepted
    places = (filled[:, None] + depths).reshape(-1)
    frequency = rope_base ** (-jnp.arange(half, dtype=f32) / half)
    angles = places.astype(f32)[:, None] * frequency[None, :]
    cosine, sine = jnp.cos(angles), jnp.sin(angles)
    cosine = jnp.concatenate([cosine, cosine], axis=1)
    sine = jnp.concatenate([-sine, sine], axis=1)

    few = rows // n_dev
    each = up(few, 16)
    tail = up(2 * turn_dim + 1, LANES)
    width = q_rank + kv_rank + tail

    def own_rows(table):
        mine = lax.dynamic_slice_in_dim(table, (me_t * n_kv + me_k) * few, few, 0)
        return jnp.pad(mine, ((0, each - few), (0, tail - turn_dim)))

    scaled = (activations.astype(f32) * gain_input.astype(f32)).astype(bf16)
    x = jnp.concatenate([scaled, activations], axis=1).reshape(n_dev, few, 2 * features)
    x = jnp.pad(x, ((0, 0), (0, each - few), (0, 0))).reshape(n_tp, n_kv * each, 2 * features)
    w = jnp.concatenate(
        [
            w_query_down,
            w_key_down,
            w_key_down[:, kv_rank + half :],
            w_key_down[:, kv_rank : kv_rank + half],
            jnp.zeros((features, tail - 2 * turn_dim), bf16),
        ],
        axis=1,
    )
    dma = pltpu.SemaphoreType.DMA
    gathered = pl.pallas_call(
        functools.partial(compress_kernel, n_kv, n_tp, width, q_rank, kv_rank, turn_dim),
        name="compress",
        out_shape=jax.ShapeDtypeStruct((n_dev, each, width), bf16),
        in_specs=[VMEM] * 6,
        out_specs=VMEM,
        scratch_shapes=[
            pltpu.VMEM((n_tp, n_kv * each, 2 * features), bf16),
            pltpu.VMEM((n_tp, features, width), bf16),
            pltpu.VMEM((n_kv, each, width), f32),
            pltpu.VMEM((n_kv, each, width), f32),
            pltpu.VMEM((n_dev, each, width), bf16),
            dma((n_tp,)), dma((n_tp,)), dma((n_tp,)), dma((n_tp,)),
            dma((n_kv,)), dma((n_kv,)),
            dma((n_dev,)), dma((n_dev,)), dma((n_dev,)),
        ],
        compiler_params=pltpu.CompilerParams(
            collective_id=0, has_side_effects=True, vmem_limit_bytes=32 * 1024 * 1024
        ),
    )(
        x, w, own_rows(cosine), own_rows(sine),
        gain_query.astype(f32)[None], gain_key.astype(f32)[None],
    )
    gathered = gathered[:, :few].reshape(rows, width)
    query_low = gathered[:, :q_rank]
    fresh = gathered[:, q_rank : q_rank + whole].reshape(seqs, props, whole).transpose(0, 2, 1)

    group = 2 if seqs % 2 == 0 else 1
    fixed = lambda *shape: pl.BlockSpec(shape, lambda i, rel: (0,) * len(shape))
    updated, part, stats = pl.pallas_call(
        functools.partial(attend_kernel, group),
        name="attend",
        out_shape=(
            jax.ShapeDtypeStruct((seqs, whole, span), bf16),
            jax.ShapeDtypeStruct((heads, rows, kv_rank), bf16),
            jax.ShapeDtypeStruct((rows, LANES), f32),
        ),
        grid_spec=pltpu.PrefetchScalarGridSpec(
            num_scalar_prefetch=1,
            grid=(seqs // group,),
            in_specs=[
                fixed(rows, q_rank),
                fixed(heads, whole, q_rank),
                fixed(rows, turn_dim),
                fixed(rows, turn_dim),
                pl.BlockSpec((group, props, props), lambda i, rel: (i, 0, 0)),
                pl.BlockSpec((group, whole, props), lambda i, rel: (i, 0, 0)),
                pl.BlockSpec((group, whole, span), lambda i, rel: (i, 0, 0)),
            ],
            out_specs=[
                pl.BlockSpec((group, whole, span), lambda i, rel: (i, 0, 0)),
                pl.BlockSpec((heads, group * props, kv_rank), lambda i, rel: (0, i, 0)),
                pl.BlockSpec((group * props, LANES), lambda i, rel: (i, 0)),
            ],
            scratch_shapes=[
                pltpu.VMEM((seqs, heads * props, kv_rank), bf16),
                pltpu.VMEM((seqs, heads * props, turn_dim), bf16),
            ],
        ),
        compiler_params=pltpu.CompilerParams(vmem_limit_bytes=48 * 1024 * 1024),
    )(
        filled - me_k * span,
        query_low,
        w_query.transpose(1, 2, 0),
        cosine,
        sine,
        reached,
        fresh,
        latent_cache.transpose(0, 2, 1),
    )

    wv = lax.dynamic_slice_in_dim(w_value.transpose(0, 2, 1), me_t * heads, heads, 0)
    per_kv, per_tp = rows // n_kv, rows // n_tp
    mixed = pl.pallas_call(
        functools.partial(project_kernel, n_kv, n_tp),
        name="project",
        out_shape=jax.ShapeDtypeStruct((n_tp, per_tp, cols), bf16),
        in_specs=[VMEM] * 5,
        out_specs=VMEM,
        scratch_shapes=[
            pltpu.VMEM((n_kv, per_kv, heads * v_dim), bf16),
            pltpu.VMEM((n_kv, per_kv, LANES), f32),
            pltpu.VMEM((n_kv, per_kv, heads * v_dim), bf16),
            pltpu.VMEM((n_kv, per_kv, LANES), f32),
            pltpu.VMEM((n_kv, per_kv, heads * v_dim), bf16),
            pltpu.VMEM((n_tp, per_tp, cols), f32),
            pltpu.VMEM((n_tp, per_tp, cols), f32),
            pltpu.VMEM((n_kv, 8, per_tp), f32),
            pltpu.VMEM((n_tp, per_tp, cols), bf16),
            dma((n_kv,)), dma((n_kv,)), dma((n_kv,)), dma((n_kv,)), dma((n_kv,)), dma((n_kv,)),
            dma((n_tp,)), dma((n_tp,)), dma((n_kv,)), dma((n_kv,)), dma((n_tp,)), dma((n_tp,)),
        ],
        compiler_params=pltpu.CompilerParams(
            collective_id=1, has_side_effects=True, vmem_limit_bytes=32 * 1024 * 1024
        ),
    )(part, stats, wv, w_out, gain_output.astype(f32)[None])
    return (mixed.reshape(rows, cols), updated.transpose(0, 2, 1))


def solution(mesh):
    in_specs = (
        P(None, ("kv", "tp")),
        P(None, "kv", None),
        P(),
        P(),
        P(),
        P(("kv", "tp"), None),
        P(("kv", "tp"), None),
        P(("kv", "tp")),
        P(),
        P(),
        P(None, "tp", None),
        P(),
        P("tp", "kv"),
        P("kv"),
    )
    out_specs = (P(None, "kv"), P(None, "kv", None))
    body = functools.partial(local, mesh.shape["kv"], mesh.shape["tp"])
    return jax.shard_map(body, mesh=mesh, in_specs=in_specs, out_specs=out_specs, check_vma=False)
```

time: 323 us -> 123 us (0.38)
  blocking collectives: 131 us -> 0 us
  Pallas kernels: 0 us -> 104 us
  waiting for transfers between devices: 83.6 us -> 0 us
  matrix products: 66.4 us -> 1.52 us
  other arithmetic: 18.6 us -> 4.7 us
  between operations: 14.7 us -> 0.85 us
  local copies, waits for them, and re-layouts: 7.89 us -> 11.2 us
    pallas_call x0 -> x3, Pallas kernels: none -> 104 us  [the longest x1 37.7 us: local(): pl.pallas_call(functools.partial(project_kernel, n_kv, n_tp), name='proje...]
    psum x2 -> x0, waiting for transfers between devices: 83.5 us -> none  [the longest x1 51.6 us: local(): lax.psum((squares, query_segment, key_segment), 'kv')]
    all_gather x5 -> x0, blocking collectives: 79.3 us -> none  [the longest x1 30.9 us: local(): lax.all_gather(totals, 'kv', axis=0, tiled=True)]
    dot_general x13 -> x2, matrix products: 66.4 us -> 1.52 us  [ancestry(): jnp.einsum('sij,sjk->sik', reached, reached, preferred_element_type=jnp.f...]
    psum x2 -> x0, blocking collectives: 43.6 us -> none  [the longest x1 22.2 us: local(): lax.psum((squares, query_segment, key_segment), 'kv')]
    reduce_sum x7 -> x0, other arithmetic: 11.3 us -> none  [the longest x1 6.87 us: partial_attend(): totals = jnp.sum(weights, axis=-1)]
    unnamed x1 -> x0, blocking collectives: 8.37 us -> none
  transfers between devices with their start and end apart: 3 -> 0, of which waited for: 2 -> 0; matrix products, arithmetic and copies ran while one was open for 3% -> 0% of each run, Pallas kernels for 0% -> 0%
where the time goes in v1:
time: 123 us; the launch traced here: 122 us
  Pallas kernels  104 us (85%)
  local copies, waits for them, and re-layouts  11.2 us (9%)
  other arithmetic  4.7 us (4%)
  matrix products  1.52 us (1%)
    pallas_call x1, Pallas kernels, local(): pl.pallas_call(functools.partial(project_kernel, n_kv, n_tp), name='proje...  37.7 us
    pallas_call x1, Pallas kernels, local(): pl.pallas_call(functools.partial(compress_kernel, n_kv, n_tp, width, q_ra...  36.3 us
    pallas_call x1, Pallas kernels, local(): pl.pallas_call(functools.partial(attend_kernel, group), name='attend', ou...  29.6 us
    unnamed x16, local copies, waits for them, and re-layouts  6.12 us

profile of v1, /device:TPU:0, one launch (start us, length us, event | category | flops | bytes accessed | tf_op | source)
XLA Modules:
  0.0 121.7 jit_solution(10298390866265433595)
XLA Ops:
  0.6 0.0 copy-start
  0.6 0.0 copy-start.6
  0.7 0.7 broadcast_subtract_fusion
  1.4 0.8 copy.26
  2.2 0.5 fusion.1
  2.7 1.0 convert_reduce_fusion
  3.7 0.1 add_convert_fusion
  3.8 0.1 convert_element_type.69
  3.9 0.2 fusion.18
  4.1 0.1 copy.29.cos_ref
  4.2 0.1 copy.30.sin_ref
  4.4 0.9 fusion.23
  5.3 0.9 concatenate.13.w_ref
  6.2 0.7 convert_element_type.58
  6.9 0.9 multiply_convert_fusion
  7.8 0.8 pad_maximum_fusion
  8.6 0.1 copy.25
  8.8 0.7 broadcast_in_dim.35
  9.5 0.7 broadcast_in_dim.36
  10.1 36.3 %compress.1 = bf16[32,16,896]{2,1,0:T(8,128)(2,1)S(1)} custom-call(bf16[4,128,128]{2,1,0:T(8,128)(2,1)S(1)} %bitcast.19, bf16[64,896]{1,0:T(8,128)(2,1)S(1)} %concatenate.13.w_ref, f32[16,128]{1,0:T(8,128)S(1)} %pad.12.cos_ref, f32[16,128]{1,0:T(8,128)S(1)} %pad.13.sin_ref, f32[1,512]{1,0:T(1,128)S(1)} %bitcast.20, f32[1,256]{1,0:T(1,128)S(1)} %bitcast.22), custom_call_target="tpu_custom_call" | custom-call | tf_op jit(solution)/shard_map/compress/pallas_call | solution.py:418
  46.4 0.2 reshape.50
  46.6 0.7 slice.21
  47.3 1.7 %copy.31 = bf16[24,16,288]{1,2,0:T(8,128)(2,1)S(1)} copy(bf16[24,16,288]{2,1,0:T(8,128)(2,1)} %bitcast.24) | data formatting | bytes 442368 | tf_op jit(solution)/shard_map/reshape | solution.py:443
  49.1 0.0 copy-start.1
  49.1 1.3 %copy-done.1 = bf16[512,4,288]{0,2,1:T(8,128)(2,1)S(1)} copy-done((bf16[512,4,288]{0,2,1:T(8,128)(2,1)S(1)}, bf16[512,4,288]{0,2,1:T(8,128)(2,1)}, u32[]{:S(2)}) %copy-start.1) | copy-done | bytes 1179672
  50.4 0.0 copy-start.5
  50.4 0.9 copy-done.5
  51.3 29.6 %attend.1 = (bf16[24,288,2048]{2,1,0:T(8,128)(2,1)}, bf16[4,384,256]{2,1,0:T(8,128)(2,1)S(1)}, f32[384,128]{1,0:T(8,128)S(1)}) custom-call(s32[24]{0:T(128)S(1)} %get-tuple-element.8.rel_ref, bf16[384,512]{1,0:T(8,128)(2,1)S(1)} %slice.20.low_ref, bf16[4,288,512]{2,1,0:T(8,128)(2,1)S(1)} %bitcast.17, f32[384,32]{1,0:T(8,128)S(1)} %copy.29.cos_ref, ...), custom_call_target="tpu_custom_call" | custom-call | tf_op jit(solution)/shard_map/attend/pallas_call | solution.py:447
  80.8 0.0 copy-start.2
  80.9 0.7 copy-done.2
  81.5 0.0 copy-done
  81.5 0.0 copy-done.6
  81.6 0.0 copy-start.3
  81.6 0.9 copy-done.3
  82.5 0.0 copy-start.4
  82.5 0.9 copy-done.4
  83.4 37.7 %project.1 = bf16[4,96,256]{2,1,0:T(8,128)(2,1)S(1)} custom-call(bf16[4,384,256]{2,1,0:T(8,128)(2,1)S(1)} %get-tuple-element.5.part_ref, f32[384,128]{1,0:T(8,128)S(1)} %copy-done.3, bf16[4,64,256]{2,1,0:T(8,128)(2,1)S(1)} %dynamic-slice_bitcast_fusion.wv_ref, bf16[256,256]{1,0:T(8,128)(2,1)S(1)} %copy-done.4, f32[1,256]{1,0:T(1,128)S(1)} %bitcast.21), custom_call_target="tpu_custom_call" | custom-call | tf_op jit(solution)/shard_map/project/pallas_call | solution.py:491
  121.1 0.7 copy.37
  (13 shorter events, 0.2 us)
Async XLA Ops:
  0.6 80.9 %copy-start = (bf16[16,256,64]{1,2,0:T(8,128)(2,1)S(1)}, bf16[16,256,64]{1,2,0:T(8,128)(2,1)}, u32[]{:S(2)}) copy-start(bf16[16,256,64]{1,2,0:T(8,128)(2,1)} %param.25) | copy-start | bytes 1572868
  0.6 80.9 %copy-start.6 = (bf16[256]{0:T(256)(128)(2,1)S(1)}, bf16[256]{0:T(256)(128)(2,1)}, u32[]{:S(2)}) copy-start(bf16[256]{0:T(256)(128)(2,1)} %param.27) | copy-start | bytes 1540
  49.1 1.3 %copy-start.1 = (bf16[512,4,288]{0,2,1:T(8,128)(2,1)S(1)}, bf16[512,4,288]{0,2,1:T(8,128)(2,1)}, u32[]{:S(2)}) copy-start(bf16[512,4,288]{0,2,1:T(8,128)(2,1)} %param.24) | copy-start | bytes 3538948
  50.4 0.9 copy-start.5
  80.8 0.7 copy-start.2
  81.6 0.9 copy-start.3
  82.5 0.9 copy-start.4

commit v2 on v1

--- a/solution.py
+++ b/solution.py
@@ -61,7 +61,7 @@
     n_kv, n_tp, width, q_rank, kv_rank, turn_dim,
     x_ref, w_ref, cos_ref, sin_ref, gain_q_ref, gain_k_ref, out_ref,
     got_x, got_w, part, got_part, all_rows,
-    send_x, recv_x, send_w, recv_w, send_p, recv_p, send_a, send_b, recv_a,
+    send_x, recv_x, send_w, recv_w, send_p, recv_p, send_a, send_y, send_b, recv_a,
 ):
     me_k, me_t = lax.axis_index("kv"), lax.axis_index("tp")
     barrier = pltpu.get_barrier_semaphore()
@@ -133,42 +133,34 @@
     all_rows[mine, :, q_rank + kv_rank :] = turned.astype(jnp.bfloat16)
 
     sibling = me_t + 1 - 2 * lax.rem(me_t, 2)
-    peers = []
-    for dy in range(n_tp // 2):
-        for dk in range(n_kv):
-            if dy or dk:
-                peers.append((lax.rem(me_k + dk, n_kv), lax.rem(me_t + 2 * dy, n_tp)))
-    for index, (pk, pt) in enumerate(peers):
-        copy = remote(
-            all_rows.at[mine], all_rows.at[mine], send_a.at[index], recv_a.at[mine],
-            {"kv": pk, "tp": pt},
-        )
+    def send(block, sem, device_id):
+        copy = remote(all_rows.at[block], all_rows.at[block], sem, recv_a.at[block], device_id)
         copy.start()
         sends.append(copy)
 
-    def pass_on(index, block):
-        copy = remote(
-            all_rows.at[block], all_rows.at[block], send_b.at[index], recv_a.at[block],
-            {"tp": sibling},
-        )
-        copy.start()
-        sends.append(copy)
-
-    pass_on(len(peers), mine)
-    for index, (pk, pt) in enumerate(peers):
-        block = pt * n_kv + pk
+    def landed(block):
         remote(
-            all_rows.at[block], all_rows.at[block], send_a.at[index], recv_a.at[block],
-            {"kv": pk, "tp": pt},
+            all_rows.at[block], all_rows.at[block], send_a.at[0], recv_a.at[block], {"tp": sibling}
         ).wait_recv()
-        pass_on(index, block)
+
+    for dk in range(1, n_kv):
+        send(mine, send_a.at[dk], {"kv": lax.rem(me_k + dk, n_kv)})
+    for dk in range(n_kv):
+        block = me_t * n_kv + lax.rem(me_k + dk, n_kv)
+        if dk:
+            landed(block)
+        for dy in range(1, n_tp // 2):
+            send(block, send_y.at[dy * n_kv + dk], {"tp": lax.rem(me_t + 2 * dy, n_tp)})
+        send(block, send_b.at[dk], {"tp": sibling})
+    for dy in range(1, n_tp // 2):
+        for dk in range(n_kv):
+            block = lax.rem(me_t + 2 * dy, n_tp) * n_kv + lax.rem(me_k + dk, n_kv)
+            landed(block)
+            send(block, send_b.at[dy * n_kv + dk], {"tp": sibling})
     for dy in range(n_tp // 2):
         for dk in range(n_kv):
             block = lax.rem(sibling + 2 * dy, n_tp) * n_kv + lax.rem(me_k + dk, n_kv)
-            remote(
-                all_rows.at[block], all_rows.at[block], send_b.at[0], recv_a.at[block],
-                {"tp": sibling},
-            ).wait_recv()
+            landed(block)
     out_ref[...] = all_rows[...]
     for copy in sends:
         copy.wait_send()
@@ -176,7 +168,7 @@
 
 def attend_kernel(
     group, rel_ref, low_ref, wq_ref, cos_ref, sin_ref, reached_ref, fresh_ref, cache_ref,
-    out_ref, part_ref, stats_ref, q_main, q_turn,
+    out_ref, part_ref, stats_ref, q_main, q_turn, bias,
 ):
     heads, whole, _ = wq_ref.shape
     turn_dim = q_turn.shape[-1]
@@ -205,6 +197,8 @@
         s = step * group + g
         rel = rel_ref[s]
         out_ref[g] = cache_ref[g]
+        past = lax.broadcasted_iota(jnp.int32, (props, span), 1) < rel
+        bias[g] = jnp.where(past, 0.0, score_after_mask)
         first = lax.shift_right_arithmetic(rel, 7)
         for more in range(2):
             chunk = first + more
@@ -214,18 +208,22 @@
                 start = pl.multiple_of(chunk * LANES, LANES)
                 slot = start - rel + lax.broadcasted_iota(jnp.int32, (props, LANES), 1)
                 onehot = slot == lax.broadcasted_iota(jnp.int32, (props, LANES), 0)
-                placed = dot(fresh_ref[g], onehot.astype(jnp.float32).astype(jnp.bfloat16))
+                onehot = onehot.astype(jnp.float32).astype(jnp.bfloat16)
+                seen = (slot < 0) | (dot(reached_ref[g], onehot) > 0.5)
+                bias[g, :, pl.ds(start, LANES)] = jnp.where(seen, 0.0, score_after_mask)
+                placed = lax.dot_general(
+                    fresh_ref[g], onehot, (((0,), (0,)), ((), ())),
+                    preferred_element_type=jnp.float32,
+                )
                 slots = start - rel + lax.broadcasted_iota(jnp.int32, placed.shape, 1)
                 old = out_ref[g, :, pl.ds(start, LANES)].astype(jnp.float32)
                 new = jnp.where((slots >= 0) & (slots < props), placed, old)
                 out_ref[g, :, pl.ds(start, LANES)] = new.astype(jnp.bfloat16)
 
-        slot = lax.broadcasted_iota(jnp.int32, (props, span), 1) - rel
-        onehot = slot == lax.broadcasted_iota(jnp.int32, (props, span), 0)
-        ancestors = dot(reached_ref[g], onehot.astype(jnp.float32).astype(jnp.bfloat16))
-        bias = jnp.where((slot < 0) | (ancestors > 0.5), 0.0, score_after_mask)
+    for g in range(group):
+        s = step * group + g
         scores = dot(q_main[s], out_ref[g, :rank, :]) + dot(q_turn[s], out_ref[g, rank:, :])
-        masked = scores.reshape(heads, props, span) * scale + bias[None]
+        masked = scores.reshape(heads, props, span) * scale + bias[g][None]
         top = jnp.max(masked, axis=-1, keepdims=True)
         weights = jnp.exp(masked - jnp.maximum(top, -1e29))
         totals = jnp.sum(weights, axis=-1, keepdims=True)
@@ -261,10 +259,15 @@
     sends = []
 
     each = vals.shape[1]
+    line = lax.broadcasted_iota(jnp.int32, (16, LANES), 0)
+    lane = lax.broadcasted_iota(jnp.int32, (16, LANES), 1)
+    tops = (line < heads) & (lane == line)
+    counts = (line >= 8) & (line < 8 + heads) & (lane == line - 8 + heads)
+    pick = jnp.where(tops | counts, 1.0, 0.0)
     values = jnp.concatenate([dot_nt(part_ref[h], wv_ref[h]) for h in range(heads)], axis=1)
     for j in range(n_kv):
         vals[j] = values[j * each : (j + 1) * each].astype(jnp.bfloat16)
-        stat[j] = stats_ref[j * each : (j + 1) * each, :]
+        stat[j] = dot_nt(pick, stats_ref[j * each : (j + 1) * each, :], HIGHEST)
     pl.semaphore_wait(barrier, n_kv + n_tp - 2)
 
     def exchange(axis, peers, src_of, dst, own, send_sem, recv_sem):
@@ -286,24 +289,25 @@
     for d in range(1, n_kv):
         arrived("kv", kv_peers, d, lambda p: stat.at[p], got_stat, send_s, recv_s)
     all_stats = [stat[me_k]] + [got_stat[p] for p in kv_peers[1:]]
-    largest = all_stats[0]
+    largest = all_stats[0][:8]
     for one in all_stats[1:]:
-        largest = jnp.maximum(largest, one)
+        largest = jnp.maximum(largest, one[:8])
+    shares = jnp.concatenate([one[8:] * jnp.exp(one[:8] - largest) for one in all_stats], axis=0)
+    turn_eye = lax.broadcasted_iota(jnp.int32, (each, each), 0) == lax.broadcasted_iota(
+        jnp.int32, (each, each), 1
+    )
+    shares = dot_nt(turn_eye.astype(jnp.float32), shares, HIGHEST)
     wide = lax.broadcasted_iota(jnp.int32, (each, heads * v_dim), 1)
 
-    def spread(share):
-        out = share[:, 0:1]
+    def spread(d):
+        out = shares[:, 8 * d : 8 * d + 1]
         for h in range(1, heads):
-            out = jnp.where(wide >= h * v_dim, share[:, h : h + 1], out)
+            out = jnp.where(wide >= h * v_dim, shares[:, 8 * d + h : 8 * d + h + 1], out)
         return jnp.broadcast_to(out, wide.shape)
 
     summed = None
     for d in range(n_kv):
-        one = all_stats[d]
-        share = pltpu.roll(one, LANES - heads, 1) * jnp.exp(
-            jnp.minimum(one - largest, 0.0)
-        )
-        share = spread(share)
+        share = spread(d)
         if d:
             arrived("kv", kv_peers, d, lambda p: vals.at[p], got_vals, send_v, recv_v)
         block = got_vals[kv_peers[d]] if d else vals[me_k]
@@ -429,7 +433,7 @@
             pltpu.VMEM((n_dev, each, width), bf16),
             dma((n_tp,)), dma((n_tp,)), dma((n_tp,)), dma((n_tp,)),
             dma((n_kv,)), dma((n_kv,)),
-            dma((n_dev,)), dma((n_dev,)), dma((n_dev,)),
+            dma((n_kv,)), dma((n_dev,)), dma((n_dev,)), dma((n_dev,)),
         ],
         compiler_params=pltpu.CompilerParams(
             collective_id=0, has_side_effects=True, vmem_limit_bytes=32 * 1024 * 1024
@@ -440,9 +444,9 @@
     )
     gathered = gathered[:, :few].reshape(rows, width)
     query_low = gathered[:, :q_rank]
-    fresh = gathered[:, q_rank : q_rank + whole].reshape(seqs, props, whole).transpose(0, 2, 1)
-
-    group = 2 if seqs % 2 == 0 else 1
+    fresh = gathered[:, q_rank : q_rank + whole].reshape(seqs, props, whole)
+
+    group = next(g for g in (3, 2, 1) if seqs % g == 0)
     fixed = lambda *shape: pl.BlockSpec(shape, lambda i, rel: (0,) * len(shape))
     updated, part, stats = pl.pallas_call(
         functools.partial(attend_kernel, group),
@@ -461,7 +465,7 @@
                 fixed(rows, turn_dim),
                 fixed(rows, turn_dim),
                 pl.BlockSpec((group, props, props), lambda i, rel: (i, 0, 0)),
-                pl.BlockSpec((group, whole, props), lambda i, rel: (i, 0, 0)),
+                pl.BlockSpec((group, props, whole), lambda i, rel: (i, 0, 0)),
                 pl.BlockSpec((group, whole, span), lambda i, rel: (i, 0, 0)),
             ],
             out_specs=[
@@ -472,6 +476,7 @@
             scratch_shapes=[
                 pltpu.VMEM((seqs, heads * props, kv_rank), bf16),
                 pltpu.VMEM((seqs, heads * props, turn_dim), bf16),
+                pltpu.VMEM((group, props, span), f32),
             ],
         ),
         compiler_params=pltpu.CompilerParams(vmem_limit_bytes=48 * 1024 * 1024),
@@ -496,9 +501,9 @@
         out_specs=VMEM,
         scratch_shapes=[
             pltpu.VMEM((n_kv, per_kv, heads * v_dim), bf16),
-            pltpu.VMEM((n_kv, per_kv, LANES), f32),
+            pltpu.VMEM((n_kv, 16, per_kv), f32),
             pltpu.VMEM((n_kv, per_kv, heads * v_dim), bf16),
-            pltpu.VMEM((n_kv, per_kv, LANES), f32),
+            pltpu.VMEM((n_kv, 16, per_kv), f32),
             pltpu.VMEM((n_kv, per_kv, heads * v_dim), bf16),
             pltpu.VMEM((n_tp, per_tp, cols), f32),
             pltpu.VMEM((n_tp, per_tp, cols), f32),

time: 123 us -> 109 us (0.89)
  Pallas kernels: 104 us -> 95.8 us
  local copies, waits for them, and re-layouts: 11.2 us -> 5.31 us
    pallas_call x1, Pallas kernels: 37.7 us -> 32.5 us  [local(): pl.pallas_call(functools.partial(project_kernel, n_kv, n_tp), name='proje...]
    pallas_call x1, Pallas kernels: 29.6 us -> 26.1 us  [local(): pl.pallas_call(functools.partial(attend_kernel, group), name='attend', ou...]
    unnamed x16 -> x10, local copies, waits for them, and re-layouts: 6.12 us -> 2.73 us
    reshape x1 -> x0, local copies, waits for them, and re-layouts: 1.74 us -> none  [local(): gathered[:, q_rank:q_rank + whole].reshape(seqs, props, whole)]
where the time goes in v2:
time: 109 us; the launch traced here: 108 us
  Pallas kernels  95.8 us (88%)
  local copies, waits for them, and re-layouts  5.31 us (5%)
  other arithmetic  4.7 us (4%)
    pallas_call x1, Pallas kernels, local(): pl.pallas_call(functools.partial(compress_kernel, n_kv, n_tp, width, q_ra...  37.2 us
    pallas_call x1, Pallas kernels, local(): pl.pallas_call(functools.partial(project_kernel, n_kv, n_tp), name='proje...  32.5 us
    pallas_call x1, Pallas kernels, local(): pl.pallas_call(functools.partial(attend_kernel, group), name='attend', ou...  26.1 us
    unnamed x10, local copies, waits for them, and re-layouts  2.73 us

profile of v2, /device:TPU:0, one launch (start us, length us, event | category | flops | bytes accessed | tf_op | source)
XLA Modules:
  0.0 107.6 jit_solution(4358962578927153205)
XLA Ops:
  0.6 0.0 copy-start
  0.6 0.0 copy-start.3
  0.7 0.0 copy-start.2
  0.7 0.7 broadcast_subtract_fusion
  1.4 0.8 copy.25
  2.2 0.5 fusion.1
  2.7 0.4 convert_reduce_fusion
  3.2 0.1 add_convert_fusion
  3.2 0.1 convert_element_type.69
  3.3 0.2 fusion.18
  3.5 0.1 copy.28.cos_ref
  3.7 0.1 copy.29.sin_ref
  3.9 0.9 fusion.23
  4.7 0.9 concatenate.13.w_ref
  5.7 0.7 convert_element_type.58
  6.3 0.9 multiply_convert_fusion
  7.2 0.8 pad_maximum_fusion
  8.0 0.1 copy.24
  8.2 0.7 broadcast_in_dim.35
  8.9 0.7 broadcast_in_dim.36
  9.6 37.2 %compress.1 = bf16[32,16,896]{2,1,0:T(8,128)(2,1)S(1)} custom-call(bf16[4,128,128]{2,1,0:T(8,128)(2,1)S(1)} %bitcast.18, bf16[64,896]{1,0:T(8,128)(2,1)S(1)} %concatenate.13.w_ref, f32[16,128]{1,0:T(8,128)S(1)} %pad.12.cos_ref, f32[16,128]{1,0:T(8,128)S(1)} %pad.13.sin_ref, f32[1,512]{1,0:T(1,128)S(1)} %bitcast.19, f32[1,256]{1,0:T(1,128)S(1)} %bitcast.21), custom_call_target="tpu_custom_call" | custom-call | tf_op jit(solution)/shard_map/compress/pallas_call | solution.py:422
  46.8 0.2 reshape.50
  47.1 0.0 copy-start.1
  47.1 1.3 %copy-done.1 = bf16[512,4,288]{0,2,1:T(8,128)(2,1)S(1)} copy-done((bf16[512,4,288]{0,2,1:T(8,128)(2,1)S(1)}, bf16[512,4,288]{0,2,1:T(8,128)(2,1)}, u32[]{:S(2)}) %copy-start.1) | copy-done | bytes 1179672
  48.3 26.1 %attend.1 = (bf16[24,288,2048]{2,1,0:T(8,128)(2,1)}, bf16[4,384,256]{2,1,0:T(8,128)(2,1)S(1)}, f32[384,128]{1,0:T(8,128)S(1)}) custom-call(s32[24]{0:T(128)S(1)} %get-tuple-element.8.rel_ref, bf16[384,512]{1,0:T(8,128)(2,1)S(1)} %slice.20.low_ref, bf16[4,288,512]{2,1,0:T(8,128)(2,1)S(1)} %bitcast.15, f32[384,32]{1,0:T(8,128)S(1)} %copy.28.cos_ref, ...), custom_call_target="tpu_custom_call" | custom-call | tf_op jit(solution)/shard_map/attend/pallas_call | solution.py:451
  74.4 0.0 copy-done
  74.4 0.0 copy-done.3
  74.5 0.0 copy-done.2
  74.5 32.5 %project.1 = bf16[4,96,256]{2,1,0:T(8,128)(2,1)S(1)} custom-call(bf16[4,384,256]{2,1,0:T(8,128)(2,1)S(1)} %get-tuple-element.5.part_ref, f32[384,128]{1,0:T(8,128)S(1)} %get-tuple-element.6.stats_ref, bf16[4,64,256]{2,1,0:T(8,128)(2,1)S(1)} %dynamic-slice_bitcast_fusion.wv_ref, bf16[256,256]{1,0:T(8,128)(2,1)S(1)} %copy-done.2, f32[1,256]{1,0:T(1,128)S(1)} %bitcast.20), custom_call_target="tpu_custom_call" | custom-call | tf_op jit(solution)/shard_map/project/pallas_call | solution.py:496
  106.9 0.7 copy.35
  (14 shorter events, 0.2 us)
Async XLA Ops:
  0.6 73.8 %copy-start = (bf16[16,256,64]{1,2,0:T(8,128)(2,1)S(1)}, bf16[16,256,64]{1,2,0:T(8,128)(2,1)}, u32[]{:S(2)}) copy-start(bf16[16,256,64]{1,2,0:T(8,128)(2,1)} %param.25) | copy-start | bytes 1572868
  0.6 73.8 %copy-start.3 = (bf16[256]{0:T(256)(128)(2,1)S(1)}, bf16[256]{0:T(256)(128)(2,1)}, u32[]{:S(2)}) copy-start(bf16[256]{0:T(256)(128)(2,1)} %param.27) | copy-start | bytes 1540
  0.7 73.8 %copy-start.2 = (bf16[256,256]{1,0:T(8,128)(2,1)S(1)}, bf16[256,256]{1,0:T(8,128)(2,1)}, u32[]{:S(2)}) copy-start(bf16[256,256]{1,0:T(8,128)(2,1)} %w_out_ref.1) | copy-start | bytes 393220
  47.1 1.3 %copy-start.1 = (bf16[512,4,288]{0,2,1:T(8,128)(2,1)S(1)}, bf16[512,4,288]{0,2,1:T(8,128)(2,1)}, u32[]{:S(2)}) copy-start(bf16[512,4,288]{0,2,1:T(8,128)(2,1)} %param.24) | copy-start | bytes 3538948
